TPU v7x, 32 devices: a whole 2x2x4 slice. The times are simulated.
32 devices in a mesh: sp: 8 (over z, x), tp: 4 (over y, core).
Axes of the slice: x: 2, y: 2, z: 4, core: 2. Of those that a mesh axis runs over, the one named last changes fastest.
Arguments:
- queries: bfloat16 [2048, 2048], P('sp', 'tp'), may hold values from -6 to 6
- keys: bfloat16 [2048, 1024], P('sp', 'tp'), may hold values from -6 to 6
- values: bfloat16 [2048, 1024], P('sp', 'tp'), may hold values from -6 to 6
- docs: int32 [2048], P('sp'), may hold values from 0 to 2, never falling along the last dimension, each value on 1 to 1280 neighbouring positions
- query_gain: float32 [64], replicated, may hold values from 0.5 to 8
- key_gain: float32 [64], replicated, may hold values from 0.5 to 8
- out_weight: bfloat16 [2048, 2048], P('tp'), may hold values from -0.125 to 0.125
- residual: bfloat16 [2048, 2048], P('sp', 'tp'), may hold values from -12 to 12
- norm_gain: float32 [2048], P('tp'), may hold values from 0.1 to 1.9
- routes: int32 [2048, 2], P('sp'), may hold values from 0 to 7, all different within a row; in each aligned block of 256 rows (0 to 255, 256 to 511, ...) at most 80 rows name the same one
- route_weight: float32 [2048, 2], P('sp'), may hold values from 0.1 to 1
- gate_weight: bfloat16 [8, 2048, 4096], P('sp', None, 'tp'), may hold values from -0.3125 to 0.3125
- up_weight: bfloat16 [8, 2048, 4096], P('sp', None, 'tp'), may hold values from -0.3125 to 0.3125
- down_weight: bfloat16 [8, 4096, 2048], P('sp', 'tp'), may hold values from -0.09375 to 0.09375
Outputs:
- mixed: bfloat16 [2048, 2048], P('sp', 'tp')
Inputs may be any that keep to these rules, and one draw needn't show every extreme that they name: `routes`: in each aligned block of 256 rows no expert is named by more than 80 rows, and 80 is reached in some block; a row names 2 different experts. `docs`: document numbers never fall along the sequence; a document holds at most 1280 positions.
All inputs are finite; a program needn't handle non-finite values.
Results may differ from a plain program's by a relative error of at most 0.028.
The roundings to bfloat16 on the way count: a program that leaves them out, or rounds other values in their place, can miss the bound.
Values may be sent and summed in bfloat16 or wider, within the bound.
A program may use at most 64 MiB of HBM per device.

v0:
```python
import jax
import jax.numpy as jnp
from jax import lax
from jax.sharding import PartitionSpec as P

GRID_W = 64


EPSILON = 1e-06
NEG_BIG = -1e30
ROTARY_BASE = 10000.0
CLAMP_LIMIT = 7.0
SIGMOID_SCALE = 1.702


def rope_tables(positions, head_dim):
    quarter = head_dim // 4
    freqs = ROTARY_BASE ** (-jnp.arange(quarter, dtype=jnp.float32) / quarter)
    row_pos = (positions // GRID_W).astype(jnp.float32)
    col_pos = (positions % GRID_W).astype(jnp.float32)
    angle = jnp.concatenate([row_pos[:, None] * freqs, col_pos[:, None] * freqs], axis=1)
    return (jnp.cos(angle), jnp.sin(angle))


def norm_rotate(heads, gain, cosine_table, sine_table):
    entries = heads.astype(jnp.float32)
    entries = (
        entries * lax.rsqrt(jnp.mean(entries * entries, axis=-1, keepdims=True) + EPSILON) * gain
    )
    pairs = entries.reshape(entries.shape[:-1] + (entries.shape[-1] // 2, 2))
    first = pairs[..., 0]
    second = pairs[..., 1]
    cos_rows = cosine_table[:, None, :]
    sin_rows = sine_table[:, None, :]
    turned = jnp.stack(
        [first * cos_rows - second * sin_rows, first * sin_rows + second * cos_rows], axis=-1
    )
    return turned.reshape(heads.shape).astype(jnp.bfloat16)


def clamped_unit(gate_pre, up_pre):
    bounded = jnp.minimum(gate_pre, CLAMP_LIMIT)
    linear = jnp.clip(up_pre, -CLAMP_LIMIT, CLAMP_LIMIT)
    return (bounded * jax.nn.sigmoid(SIGMOID_SCALE * bounded) * (linear + 1.0)).astype(jnp.bfloat16)


def block_length(length):
    block_size = length
    while block_size > 2048 and block_size % 2 == 0:
        block_size = block_size // 2
    return block_size


def softmax_update(running, inputs, query_rot, own_tags, score_scale):
    row_peak, denominator, carried = running
    key_block, value_block, tag_block = inputs
    scores = (
        jnp.einsum("tkgd,pkd->tkgp", query_rot, key_block, preferred_element_type=jnp.float32)
        * score_scale
    )
    allowed = own_tags[:, None, None, None] == tag_block[None, None, None, :]
    scores = jnp.where(allowed, scores, NEG_BIG)
    new_peak = jnp.maximum(row_peak, jnp.max(scores, axis=-1))
    weights = jnp.where(allowed, jnp.exp(scores - new_peak[..., None]), 0.0)
    factor = jnp.exp(row_peak - new_peak)
    denominator = denominator * factor + jnp.sum(weights, axis=-1)
    carried = carried * factor[..., None] + jnp.einsum(
        "tkgp,pkd->tkgd",
        weights.astype(jnp.bfloat16),
        value_block,
        preferred_element_type=jnp.float32,
    )
    return (new_peak, denominator, carried)


def per_device(
    queries,
    keys,
    values,
    docs,
    query_gain,
    key_gain,
    out_weight,
    residual,
    norm_gain,
    routes,
    route_weight,
    gate_weight,
    up_weight,
    down_weight,
):
    tokens = queries.shape[0]
    head_dim = query_gain.shape[0]
    query_heads = queries.shape[1] // head_dim
    pair_heads = keys.shape[1] // head_dim
    pair_width = keys.shape[1]
    positions = lax.axis_index("sp") * tokens + jnp.arange(tokens, dtype=jnp.int32)
    cosine_table, sine_table = rope_tables(positions, head_dim)
    query_rot = norm_rotate(
        queries.reshape(tokens, query_heads, head_dim), query_gain, cosine_table, sine_table
    )
    query_rot = query_rot.reshape(tokens, pair_heads, 2, head_dim)
    key_rot = norm_rotate(
        keys.reshape(tokens, pair_heads, head_dim), key_gain, cosine_table, sine_table
    )
    stacked = jnp.concatenate([key_rot.reshape(tokens, pair_width), values], axis=1)
    own_tags = docs.astype(jnp.bfloat16)
    score_scale = head_dim ** (-0.5)
    stat_shape = (tokens, pair_heads, 2)
    initial = (
        jnp.full(stat_shape, NEG_BIG, jnp.float32),
        jnp.zeros(stat_shape, jnp.float32),
        jnp.zeros(stat_shape + (head_dim,), jnp.float32),
    )
    pair_rows = lax.all_gather(stacked, "sp", axis=0, tiled=True)
    tag_rows = lax.all_gather(own_tags, "sp", axis=0, tiled=True)
    length = pair_rows.shape[0]
    block_size = block_length(length)
    blocks = length // block_size
    key_part = pair_rows[:, :pair_width].reshape(blocks, block_size, pair_heads, head_dim)
    value_part = pair_rows[:, pair_width:].reshape(blocks, block_size, pair_heads, head_dim)
    tag_part = tag_rows.reshape(blocks, block_size)

    def advance(carry_state, inputs):
        return (softmax_update(carry_state, inputs, query_rot, own_tags, score_scale), None)

    result, _ = lax.scan(advance, initial, (key_part, value_part, tag_part))
    row_peak, denominator, carried = result
    attended = (
        (carried / denominator[..., None])
        .astype(jnp.bfloat16)
        .reshape(tokens, query_heads * head_dim)
    )
    width_local = residual.shape[1]
    projected = lax.psum_scatter(
        lax.dot_general(
            out_weight, attended, (((0,), (1,)), ((), ())), preferred_element_type=jnp.float32
        ).astype(jnp.bfloat16),
        "tp",
        scatter_dimension=0,
        tiled=True,
    ).astype(jnp.float32)
    mixed_first = residual.astype(jnp.float32) + projected.T
    squares = lax.psum(jnp.sum(mixed_first * mixed_first, axis=1), "tp")
    full_width = width_local * lax.axis_size("tp")
    normed = (mixed_first * lax.rsqrt(squares / full_width + EPSILON)[:, None] * norm_gain).astype(
        jnp.bfloat16
    )
    experts = lax.axis_size("sp")
    top_count = routes.shape[1]
    capacity = max(2, 5 * tokens * top_count // (4 * experts))
    flat_routes = routes.reshape(-1)
    entries = flat_routes.shape[0]
    expert_ids = jnp.arange(experts, dtype=jnp.int32)
    onehot = (flat_routes[:, None] == expert_ids[None, :]).astype(jnp.int32)
    earlier = jnp.cumsum(onehot, axis=0) - onehot
    slot_index = jnp.sum(earlier * onehot, axis=1)
    slot_ids = jnp.arange(capacity, dtype=jnp.int32)
    matches = (flat_routes[:, None, None] == expert_ids[None, :, None]) & (
        slot_index[:, None, None] == slot_ids[None, None, :]
    )
    entry_ids = jnp.arange(entries, dtype=jnp.int32)
    source_entry = jnp.sum(jnp.where(matches, entry_ids[:, None, None], 0), axis=0)
    occupied = jnp.any(matches, axis=0)
    source_row = source_entry // top_count
    gate_local = gate_weight[0]
    up_local = up_weight[0]
    down_local = down_weight[0]
    model_width = gate_local.shape[0]
    outgoing = jnp.where(occupied[..., None], normed[source_row], jnp.zeros((), jnp.bfloat16))
    arrived = lax.all_to_all(outgoing, "sp", split_axis=0, concat_axis=0, tiled=True)
    sources = arrived.shape[0]
    flat_rows = arrived.reshape(-1, width_local)
    column_piece = lax.all_gather(flat_rows, "tp", axis=1, tiled=True)
    gate_pre = jnp.dot(column_piece, gate_local, preferred_element_type=jnp.float32)
    up_pre = jnp.dot(column_piece, up_local, preferred_element_type=jnp.float32)
    hidden = clamped_unit(gate_pre, up_pre)
    partial_value = jnp.dot(hidden, down_local, preferred_element_type=jnp.float32).reshape(
        sources, capacity, model_width
    )
    expert_out = lax.psum_scatter(
        partial_value.astype(jnp.bfloat16), "tp", scatter_dimension=2, tiled=True
    )
    returned = lax.all_to_all(expert_out, "sp", split_axis=0, concat_axis=0, tiled=True)
    lookup = flat_routes * capacity + slot_index
    picked = (
        returned.reshape(-1, width_local)[lookup]
        .reshape(tokens, top_count, width_local)
        .astype(jnp.float32)
    )
    routed = jnp.sum(route_weight[:, :, None] * picked, axis=1)
    return (mixed_first + routed).astype(jnp.bfloat16)


def solution(mesh):
    in_specs = (
        P("sp", "tp"),
        P("sp", "tp"),
        P("sp", "tp"),
        P("sp"),
        P(),
        P(),
        P("tp", None),
        P("sp", "tp"),
        P("tp"),
        P("sp", None),
        P("sp", None),
        P("sp", None, "tp"),
        P("sp", None, "tp"),
        P("sp", "tp", None),
    )
    out_specs = P("sp", "tp")
    return jax.shard_map(
        per_device, mesh=mesh, in_specs=in_specs, out_specs=out_specs, check_vma=False
    )
```

profile of v0, /device:TPU:0, one launch (start us, length us, event | category | flops | bytes accessed | tf_op | source)
XLA Modules:
  0.0 244.0 jit_solution(5147437151146860078)
XLA Ops:
  6.5 1.2 copy.40
  7.7 0.1 reshape.362
  7.9 1.0 copy.41
  8.9 0.8 mul.239
  9.7 0.1 broadcast_multiply_fusion.1
  9.8 0.1 fusion.32
  9.9 0.2 multiply_multiply_fusion.1
  10.1 0.3 subtract_convert_fusion.1
  10.5 0.3 pad_maximum_fusion.2
  10.8 0.1 convert_element_type.96
  10.8 0.7 pad_maximum_fusion
  11.5 0.0 all-gather.4.cloned.1.call-update
  11.6 0.0 reduce-scatter.3.cloned.1.call-start
  11.6 0.7 convert_element_type.90
  12.3 22.4 %all-gather = bf16[8,1,256]{2,1,0:T(2,128)(2,1)S(1)} all-gather(bf16[1,1,256]{2,1,0:T(2,128)(2,1)S(1)} %reshape.382), channel_id=1, replica_groups=mesh['sp'=8,'tp'=4] {'sp'}, dimensions={0}, use_global_device_ids=true | all-gather | bytes 4608 | tf_op jit(solution)/shard_map/all_gather | solution.py:116
  34.7 1.1 copy.42
  35.8 0.3 reshape.363
  36.1 0.1 mul.258
  36.2 0.1 bitcast_reduce_fusion
  36.3 0.3 multiply_multiply_fusion
  36.6 0.7 subtract_convert_fusion
  37.2 0.6 pad_maximum_fusion.1
  37.9 0.1 convert_element_type.100
  38.0 0.4 broadcast_compare_fusion
  38.4 26.5 %all-gather.4.cloned.1.call-done = bf16[2048,512]{0,1:T(8,128)(2,1)} async-done(((bf16[256,512]{0,1:T(8,128)(2,1)}), bf16[2048,512]{0,1:T(8,128)(2,1)}) %all-gather.4.cloned.1.call-update) | async-done | bytes 2097168 | tf_op jit(solution)/shard_map/all_gather | solution.py:115
  64.8 1.7 fusion.46
  66.5 2.6 %fusion = (f32[256,4,2]{0,2,1:T(2,128)S(1)}, f32[4,2048,256,2]{2,1,3,0:T(8,128)S(1)}) fusion(pred[256,2048]{0,1:T(8,128)(4,1)S(1)} %broadcast_compare_fusion, bf16[2048,4,64,1]{0,2,3,1:T(8,128)(2,1)S(1)} %bitcast.120, bf16[256,4,2,64]{0,3,2,1:T(8,128)(2,1)S(1)} %convert_element_type.100), kind=kOutput, calls=%fused_computation.4 | convolution fusion | flops 549451776 | bytes 18620416 | tf_op jit(solution)/shard_map/while/body/eval_jaxpr/tkgd,pkd->tkgp/dot_general | solution.py:58
  69.1 4.0 %fusion.1 = f32[256,4,2]{0,2,1:T(2,128)S(1)} fusion(f32[4,2048,256,2]{2,1,3,0:T(8,128)S(1)} %get-tuple-element.45, f32[256,4,2]{0,2,1:T(2,128)S(1)} %broadcast_maximum_fusion, pred[256,2048]{0,1:T(8,128)(4,1)S(1)} %broadcast_compare_fusion), kind=kLoop, calls=%fused_computation.5 | loop fusion | flops 20969472 | bytes 17317888 | tf_op jit(solution)/shard_map/while/body/eval_jaxpr/reduce_sum | solution.py:66
  73.2 3.9 %fusion.28 = bf16[256,4,2,64]{0,3,2,1:T(8,128)(2,1)S(1)} fusion(bf16[2048,4,64,1]{0,2,3,1:T(8,128)(2,1)S(1)} %bitcast.119, f32[4,2048,256,2]{2,1,3,0:T(8,128)S(1)} %get-tuple-element.45, f32[256,4,2]{0,2,1:T(2,128)S(1)} %broadcast_maximum_fusion, pred[256,2048]{0,1:T(8,128)(4,1)S(1)} %broadcast_compare_fusion, f32[256,4,2]{0,2,1:T(2,128)S(1)} %get-tuple-element.41, ...), kind=kOutput, calls=%fused_computation.26 | convolution fusion | flops 558235648 | bytes 18636800 | tf_op jit(solution)/shard_map/while/body/eval_jaxpr/tkgp,pkd->tkgd/dot_general | solution.py:67
  77.2 1.7 fusion.15
  78.9 0.0 reduce-scatter.3.cloned.1.call-update
  78.9 0.2 all-gather.6.cloned.1.call-start
  79.2 0.1 copy.45
  79.3 0.1 eq.89
  79.5 0.1 eq.85
  79.6 1.1 reduce-window.6
  80.8 0.2 slice_reduce_fusion
  81.0 0.1 fusion.34
  81.2 0.3 fusion.18
  81.5 0.1 reshape.367
  81.6 0.2 and_reduce_fusion
  81.8 20.3 %reduce-scatter.3.cloned.1.call-done = bf16[512,256]{0,1:T(8,128)(2,1)} async-done(((bf16[2048,256]{0,1:T(8,128)(2,1)}), bf16[512,256]{0,1:T(8,128)(2,1)}) %reduce-scatter.3.cloned.1.call-update) | async-done | bytes 262160 | tf_op jit(solution)/shard_map/reduce_scatter | solution.py:135
  102.1 1.1 multiply_reduce_fusion.1
  103.2 5.8 %psum.7 = f32[256]{0:T(256)S(1)} all-reduce(f32[256]{0:T(256)S(1)} %multiply_reduce_fusion.1), channel_id=1, replica_groups=mesh['sp'=8,'tp'=4] {'tp'}, use_global_device_ids=true, to_apply=%region_10.11 | all-reduce | flops 256 | bytes 2048 | tf_op jit(solution)/shard_map/psum | solution.py:144
  109.0 1.1 multiply_convert_fusion.1
  110.1 2.8 %gather_fusion = bf16[640,512]{1,0:T(8,128)(2,1)S(1)} fusion(bf16[256,512]{1,0:T(8,128)(2,1)S(1)} %multiply_convert_fusion.1, s32[1024]{0:T(1024)S(1)} %pad_clamp_fusion.1), kind=kCustom, calls=%fused_computation | custom fusion | bytes 1313280 | tf_op jit(solution)/shard_map/gather | solution.py:170
  112.9 0.2 broadcast_select_fusion
  113.0 23.1 %all_to_all.10 = bf16[8,80,512]{2,1,0:T(8,128)(2,1)} all-to-all(bf16[8,80,512]{2,1,0:T(8,128)(2,1)S(1)} %broadcast_select_fusion), channel_id=1, replica_groups=mesh['sp'=8,'tp'=4] {'sp'}, dimensions={0} | all-to-all | bytes 1310720 | tf_op jit(solution)/shard_map/all_to_all | solution.py:171
  136.1 0.0 all-gather.6.cloned.1.call-update
  136.1 0.0 reduce-scatter.5.cloned.1.call-start
  136.2 23.3 %all-gather.6.cloned.1.call-done = bf16[640,2048]{1,0:T(8,128)(2,1)} async-done(((bf16[640,512]{1,0:T(8,128)(2,1)}), bf16[640,2048]{1,0:T(8,128)(2,1)}) %all-gather.6.cloned.1.call-update) | async-done | bytes 2621456 | tf_op jit(solution)/shard_map/all_gather | solution.py:174
  159.5 5.6 %fusion.8 = f32[640,1024]{1,0:T(8,128)S(1)} fusion(bf16[640,2048]{1,0:T(8,128)(2,1)} %all-gather.6.cloned.1.call-done, bf16[1,2048,1024]{2,1,0:T(8,128)(2,1)} %param.26), kind=kOutput, calls=%fused_computation.11 | convolution fusion | flops 2684354560 | bytes 9437184 | tf_op jit(solution)/shard_map/dot_general | solution.py:176
  165.1 3.5 %multiply_convert_fusion = bf16[640,1024]{1,0:T(8,128)(2,1)S(1)} fusion(f32[640,1024]{1,0:T(8,128)S(1)} %fusion.8, bf16[640,2048]{1,0:T(8,128)(2,1)S(1)} %copy-done.8, bf16[1,2048,1024]{2,1,0:T(8,128)(2,1)S(1)} %copy-done.6), kind=kOutput, calls=%fused_computation.16 | convolution fusion | flops 2690908160 | bytes 10747904 | tf_op jit(solution)/shard_map/dot_general | solution.py:175
  168.7 4.2 %fusion.12 = bf16[8,80,2048]{2,1,0:T(8,128)(2,1)} fusion(bf16[8,80,1024]{2,1,0:T(8,128)(2,1)S(1)} %bitcast.126, bf16[1,1024,2048]{2,1,0:T(8,128)(2,1)S(1)} %copy-done.7), kind=kOutput, calls=%fused_computation.15 | convolution fusion | flops 2685665280 | bytes 8126464 | tf_op jit(solution)/shard_map/dot_general | solution.py:178
  172.9 34.5 %reduce-scatter.5.cloned.1.call-done = bf16[8,80,512]{2,1,0:T(8,128)(2,1)} async-done(((bf16[8,80,2048]{2,1,0:T(8,128)(2,1)}), bf16[8,80,512]{2,1,0:T(8,128)(2,1)}) %reduce-scatter.5.cloned.1.call-update) | async-done | bytes 655376 | tf_op jit(solution)/shard_map/reduce_scatter | solution.py:181
  207.4 5.5 %all-to-all-start.1 = ((bf16[8,80,512]{2,1,0:T(8,128)(2,1)}), bf16[8,80,512]{2,1,0:T(8,128)(2,1)S(1)}, u32[]{:S(2)}, u32[]{:S(2)}) async-start(bf16[8,80,512]{2,1,0:T(8,128)(2,1)} %reduce-scatter.5.cloned.1.call-done), calls=%async_computation.3 | async-start | bytes 1310720 | tf_op jit(solution)/shard_map/all_to_all | solution.py:184
  212.9 0.1 copy.47
  213.1 0.1 mul.284
  213.2 0.1 copy.44
  213.4 16.7 %all-to-all-done.1 = bf16[8,80,512]{2,1,0:T(8,128)(2,1)S(1)} async-done(((bf16[8,80,512]{2,1,0:T(8,128)(2,1)}), bf16[8,80,512]{2,1,0:T(8,128)(2,1)S(1)}, u32[]{:S(2)}, u32[]{:S(2)}) %all-to-all-start.1) | async-done | bytes 655392 | tf_op jit(solution)/shard_map/all_to_all | solution.py:184
  230.0 2.6 %gather_fusion.1 = bf16[512,512]{1,0:T(8,128)(2,1)} fusion(bf16[640,512]{1,0:T(8,128)(2,1)S(1)} %bitcast.116, s32[1024]{0:T(1024)S(1)} %pad_clamp_fusion), kind=kCustom, calls=%fused_computation.1 | custom fusion | bytes 1050624 | tf_op jit(solution)/shard_map/gather | solution.py:187
  232.7 1.7 reshape.364
  234.4 1.3 multiply_reduce_fusion
  235.7 1.8 add_convert_fusion
  (41 shorter events, 0.3 us)
Async XLA Ops:
  6.5 70.7 %copy-start = (bf16[512,2048]{1,0:T(8,128)(2,1)S(1)}, bf16[512,2048]{1,0:T(8,128)(2,1)}, u32[]{:S(2)}) copy-start(bf16[512,2048]{1,0:T(8,128)(2,1)} %param.20) | copy-start | bytes 6291460
  6.5 29.6 %copy-start.5 = (f32[64]{0:T(128)S(1)}, f32[64]{0:T(128)}, u32[]{:S(2)}) copy-start(f32[64]{0:T(128)} %param.18) | copy-start | bytes 772
  6.5 58.3 %all-gather.4.cloned.1.call-start = ((), (), s32[]{:S(2)}) async-start(), calls=%async_computation.4 | async-start | bytes 2359296 | tf_op jit(solution)/shard_map/all_gather | solution.py:115
  11.6 90.5 %reduce-scatter.3.cloned.1.call-start = ((), (), s32[]{:S(2)}) async-start(), calls=%async_computation.5 | async-start | bytes 1310720 | tf_op jit(solution)/shard_map/reduce_scatter | solution.py:135
  77.2 2.0 copy-start.2
  77.2 24.9 %copy-start.1 = (bf16[256,512]{1,0:T(8,128)(2,1)S(1)}, bf16[256,512]{1,0:T(8,128)(2,1)}, u32[]{:S(2)}) copy-start(bf16[256,512]{1,0:T(8,128)(2,1)} %param.21) | copy-start | bytes 786436
  77.2 31.8 %copy-start.3 = (f32[512]{0:T(512)S(1)}, f32[512]{0:T(512)}, u32[]{:S(2)}) copy-start(f32[512]{0:T(512)} %param.22) | copy-start | bytes 6148
  78.9 80.6 %all-gather.6.cloned.1.call-start = ((), (), s32[]{:S(2)}) async-start(), calls=%async_computation.6 | async-start | bytes 3276800 | tf_op jit(solution)/shard_map/all_gather | solution.py:174
  136.1 71.3 %reduce-scatter.5.cloned.1.call-start = ((), (), s32[]{:S(2)}) async-start(), calls=%async_computation.7 | async-start | bytes 3276800 | tf_op jit(solution)/shard_map/reduce_scatter | solution.py:181
  159.5 5.6 %copy-start.6 = (bf16[1,2048,1024]{2,1,0:T(8,128)(2,1)S(1)}, bf16[1,2048,1024]{2,1,0:T(8,128)(2,1)}, u32[]{:S(2)}) copy-start(bf16[1,2048,1024]{2,1,0:T(8,128)(2,1)} %param.25) | copy-start | bytes 12582916
  159.5 5.6 %copy-start.8 = (bf16[640,2048]{1,0:T(8,128)(2,1)S(1)}, bf16[640,2048]{1,0:T(8,128)(2,1)}, u32[]{:S(2)}) copy-start(bf16[640,2048]{1,0:T(8,128)(2,1)} %all-gather.6.cloned.1.call-done) | copy-start | bytes 7864324
  165.1 3.6 %copy-start.7 = (bf16[1,1024,2048]{2,1,0:T(8,128)(2,1)S(1)}, bf16[1,1024,2048]{2,1,0:T(8,128)(2,1)}, u32[]{:S(2)}) copy-start(bf16[1,1024,2048]{2,1,0:T(8,128)(2,1)} %param.27) | copy-start | bytes 12582916
  172.9 40.3 %copy-start.4 = (f32[256,2]{0,1:T(2,128)S(1)}, f32[256,2]{0,1:T(2,128)}, u32[]{:S(2)}) copy-start(f32[256,2]{0,1:T(2,128)} %param.24) | copy-start | bytes 6148
  207.4 22.6 %all-to-all-start.1 = ((bf16[8,80,512]{2,1,0:T(8,128)(2,1)}), bf16[8,80,512]{2,1,0:T(8,128)(2,1)S(1)}, u32[]{:S(2)}, u32[]{:S(2)}) async-start(bf16[8,80,512]{2,1,0:T(8,128)(2,1)} %reduce-scatter.5.cloned.1.call-done), calls=%async_computation.3 | async-start | bytes 1310720 | tf_op jit(solution)/shard_map/all_to_all | solution.py:184
Sparse Core Ops, SparseCore 0:
  11.7 53.0 all-gather.3
  79.1 22.9 reduce-scatter.2
  136.2 23.2 all-gather.5
  173.0 34.3 reduce-scatter.4
where the time goes:
time: 245 us; the launch traced here: 244 us
  waiting for transfers between devices  121 us (49%)
  blocking collectives  51.2 us (21%)
  matrix products  21.6 us (9%)
  other arithmetic  15.9 us (6%)
  local copies, waits for them, and re-layouts  14.6 us (6%)
  between operations  13.6 us (6%)
  starting transfers between devices  5.82 us (2%)
    reduce_scatter x1, waiting for transfers between devices, per_device(): lax.psum_scatter(partial_value.astype(jnp.bfloat16), 'tp', scatter_dimens...  34.5 us
    all_gather x1, waiting for transfers between devices, per_device(): pair_rows = lax.all_gather(stacked, 'sp', axis=0, tiled=True)  26.5 us
    all_gather x1, waiting for transfers between devices, per_device(): column_piece = lax.all_gather(flat_rows, 'tp', axis=1, tiled=True)  23.3 us
    all_to_all x1, blocking collectives, per_device(): lax.all_to_all(outgoing, 'sp', split_axis=0, concat_axis=0, tiled=True)  23.1 us
    all_gather x1, blocking collectives, per_device(): tag_rows = lax.all_gather(own_tags, 'sp', axis=0, tiled=True)  22.4 us
    reduce_scatter x1, waiting for transfers between devices, per_device(): lax.psum_scatter(lax.dot_general(out_weight, attended, (((0,), (1,)), (()...  20.3 us
    all_to_all x1, waiting for transfers between devices, per_device(): lax.all_to_all(expert_out, 'sp', split_axis=0, concat_axis=0, tiled=True)  16.7 us
    psum x1, blocking collectives, per_device(): squares = lax.psum(jnp.sum(mixed_first * mixed_first, axis=1), 'tp')  5.76 us
  transfers between devices with their start and end apart: 5, of which 5 were waited for; matrix products, arithmetic and copies ran while one was open for 3% of the time, Pallas kernels for 0%

commit v1 on v0

--- a/solution.py
+++ b/solution.py
@@ -1,6 +1,10 @@
+import functools
+
 import jax
 import jax.numpy as jnp
 from jax import lax
+from jax.experimental import pallas as pl
+from jax.experimental.pallas import tpu as pltpu
 from jax.sharding import PartitionSpec as P
 
 GRID_W = 64
@@ -71,6 +75,392 @@
         preferred_element_type=jnp.float32,
     )
     return (new_peak, denominator, carried)
+
+
+MESH = pl.DeviceIdType.MESH
+VMEM_SPEC = pl.BlockSpec(memory_space=pltpu.VMEM)
+VMEM_LIMIT = 56 * 1024 * 1024
+
+
+def remote(src, dst, send_sem, recv_sem, device):
+    return pltpu.make_async_remote_copy(
+        src_ref=src,
+        dst_ref=dst,
+        send_sem=send_sem,
+        recv_sem=recv_sem,
+        device_id=device,
+        device_id_type=MESH,
+    )
+
+
+def enter(devices):
+    barrier = pltpu.get_barrier_semaphore()
+    for device in devices:
+        pl.semaphore_signal(barrier, inc=1, device_id=device, device_id_type=MESH)
+    pl.semaphore_wait(barrier, len(devices))
+
+
+def call(kernel, out_shape, scratch, collective, *args):
+    return pl.pallas_call(
+        kernel,
+        out_shape=out_shape,
+        in_specs=[VMEM_SPEC] * len(args),
+        out_specs=jax.tree.map(lambda _: VMEM_SPEC, out_shape),
+        scratch_shapes=scratch,
+        compiler_params=pltpu.CompilerParams(
+            collective_id=collective, has_side_effects=True, vmem_limit_bytes=VMEM_LIMIT
+        ),
+    )(*args)
+
+
+def ring_index(place, n):
+    upper = place // (n // 2)
+    return (1 - upper) * 2 * place + upper * (2 * (n - 1 - place) + 1)
+
+
+def gather_kernel(n, pieces, kv_ref, doc_ref, kv_out, doc_out, send, recv, doc_send, doc_recv):
+    me, tp = lax.axis_index("sp"), lax.axis_index("tp")
+    odd = me % 2
+    place = (1 - odd) * (me // 2) + odd * (n - 1 - me // 2)
+    right = (ring_index((place + 1) % n, n), tp)
+    left = (ring_index((place + n - 1) % n, n), tp)
+    enter([((me + d) % n, tp) for d in range(1, n)])
+    rows = kv_ref.shape[0] // (2 * pieces)
+    copies = []
+
+    def hop(step, chunk):
+        forward = chunk < pieces
+        origin = (place - step + n) % n if forward else (place + step) % n
+        block = ring_index(origin, n)
+        span = pl.ds(chunk * rows, rows)
+        src = kv_ref.at[span] if step == 0 else kv_out.at[block, span]
+        copy = remote(
+            src, kv_out.at[block, span], send.at[chunk, step], recv.at[chunk, step],
+            right if forward else left,
+        )
+        copy.start()
+        return copy
+
+    order = [c for p in range(pieces) for c in (p, pieces + p)]
+    flying = {c: hop(0, c) for c in order}
+    doc_copies = []
+    for d in range(1, n):
+        copy = remote(
+            doc_ref, doc_out.at[me], doc_send.at[d], doc_recv.at[d], ((me + d) % n, tp)
+        )
+        copy.start()
+        doc_copies.append(copy)
+    kv_out[me] = kv_ref[...]
+    doc_out[me] = doc_ref[...]
+    for step in range(1, n):
+        for c in order:
+            flying[c].wait_recv()
+            copies.append(flying[c])
+            if step < n - 1:
+                flying[c] = hop(step, c)
+    for copy in copies:
+        copy.wait_send()
+    for copy in doc_copies:
+        copy.wait()
+
+
+def gather_blocks(kv, docs, n):
+    tokens, width = kv.shape
+    pieces = 2
+    tags = jnp.broadcast_to(docs[None, :], (8, tokens))
+    return call(
+        functools.partial(gather_kernel, n, pieces),
+        (
+            jax.ShapeDtypeStruct((n, tokens, width), kv.dtype),
+            jax.ShapeDtypeStruct((n, 8, tokens), tags.dtype),
+        ),
+        [
+            pltpu.SemaphoreType.DMA((2 * pieces, n)),
+            pltpu.SemaphoreType.DMA((2 * pieces, n)),
+            pltpu.SemaphoreType.DMA((n,)),
+            pltpu.SemaphoreType.DMA((n,)),
+        ],
+        0,
+        kv,
+        tags,
+    )
+
+
+def tp_columns(index, width):
+    return pl.ds(pl.multiple_of(index * width, width), width)
+
+
+def norm_kernel(
+    tp_size, part_ref, res_ref, gain_ref, mixed_ref, normed_ref,
+    near, outbox, far, sums, sums_in, near_s, near_r, far_s, far_r, sum_s, sum_r,
+):
+    sp, me = lax.axis_index("sp"), lax.axis_index("tp")
+    ys = tp_size // 2
+    y, core = me // 2, me % 2
+    partner = (sp, y * 2 + 1 - core)
+    width = res_ref.shape[1]
+    enter([(sp, (me + d) % tp_size) for d in range(1, tp_size)])
+    order = list(range(1, ys)) + [0]
+    near_copies = {}
+    for dy in order:
+        cols = tp_columns(((y + dy) % ys) * 2 + 1 - core, width)
+        near_copies[dy] = remote(
+            part_ref.at[:, cols], near.at[dy], near_s.at[dy], near_r.at[dy], partner
+        )
+        near_copies[dy].start()
+    far_copies = []
+    for dy in range(1, ys):
+        near_copies[dy].wait_recv()
+        own = part_ref[:, tp_columns(((y + dy) % ys) * 2 + core, width)]
+        outbox[dy] = (own.astype(jnp.float32) + near[dy].astype(jnp.float32)).astype(jnp.bfloat16)
+        copy = remote(
+            outbox.at[dy], far.at[dy], far_s.at[dy], far_r.at[dy],
+            (sp, ((y + dy) % ys) * 2 + core),
+        )
+        copy.start()
+        far_copies.append(copy)
+    near_copies[0].wait_recv()
+    total = res_ref[...].astype(jnp.float32) + (
+        part_ref[:, tp_columns(me, width)].astype(jnp.float32) + near[0].astype(jnp.float32)
+    )
+    for dy in range(1, ys):
+        far_copies[dy - 1].wait_recv()
+        total = total + far[dy].astype(jnp.float32)
+    mixed_ref[...] = total
+    square = jnp.sum(total * total, axis=1, keepdims=True)
+    square = jnp.broadcast_to(square, (square.shape[0], 128)).T
+    sums[...] = square[0:8]
+    sum_copies = []
+    for d in range(1, tp_size):
+        copy = remote(
+            sums, sums_in.at[d], sum_s.at[d], sum_r.at[d], (sp, (me + d) % tp_size)
+        )
+        copy.start()
+        sum_copies.append(copy)
+    full = square[0:8]
+    for d in range(1, tp_size):
+        sum_copies[d - 1].wait_recv()
+        full = full + sums_in[d]
+    scale = lax.rsqrt(full / (width * tp_size) + EPSILON)
+    scale = jnp.broadcast_to(scale[0:1], (128, full.shape[1])).T[:, 0:1]
+    normed_ref[...] = (mixed_ref[...] * scale * gain_ref[...]).astype(jnp.bfloat16)
+    for copy in list(near_copies.values()) + far_copies + sum_copies:
+        copy.wait_send()
+
+
+def reduce_and_norm(part, residual, gain, tp_size):
+    tokens, width = residual.shape
+    ys = tp_size // 2
+    block = (ys, tokens, width)
+    return call(
+        functools.partial(norm_kernel, tp_size),
+        (
+            jax.ShapeDtypeStruct((tokens, width), jnp.float32),
+            jax.ShapeDtypeStruct((tokens, width), jnp.bfloat16),
+        ),
+        [
+            pltpu.VMEM(block, jnp.bfloat16),
+            pltpu.VMEM(block, jnp.bfloat16),
+            pltpu.VMEM(block, jnp.bfloat16),
+            pltpu.VMEM((8, tokens), jnp.float32),
+            pltpu.VMEM((tp_size, 8, tokens), jnp.float32),
+        ]
+        + [pltpu.SemaphoreType.DMA((ys,))] * 4
+        + [pltpu.SemaphoreType.DMA((tp_size,))] * 2,
+        1,
+        part,
+        residual,
+        gain.reshape(1, width),
+    )
+
+
+def dispatch_kernel(
+    n, tp_size, out_ref, rows_ref, hop_s, hop_r, far_s, far_r, near_s, near_r, pass_s, pass_r
+):
+    me, tp = lax.axis_index("sp"), lax.axis_index("tp")
+    ys = tp_size // 2
+    y, core = tp // 2, tp % 2
+    partner = (me, y * 2 + 1 - core)
+    width = out_ref.shape[2]
+    mine = tp_columns(tp, width)
+    enter(
+        [((me + d) % n, tp) for d in range(1, n)]
+        + [(me, ((y + dy) % ys) * 2 + core) for dy in range(1, ys)]
+        + [partner]
+    )
+
+    def hop(d):
+        peer = (me + d) % n
+        return remote(
+            out_ref.at[peer], rows_ref.at[me, :, mine], hop_s.at[d], hop_r.at[d], (peer, tp)
+        )
+
+    def far(d, dy):
+        block = (me - d + n) % n
+        view = rows_ref.at[block, :, mine]
+        return remote(
+            view, view, far_s.at[d, dy], far_r.at[d, dy], (me, ((y + dy) % ys) * 2 + core)
+        )
+
+    def near(d):
+        view = rows_ref.at[(me - d + n) % n, :, mine]
+        return remote(view, view, near_s.at[d], near_r.at[d], partner)
+
+    def forward(d, dy):
+        origin = ((y - dy + ys) % ys) * 2 + core
+        view = rows_ref.at[(me - d + n) % n, :, tp_columns(origin, width)]
+        return remote(view, view, pass_s.at[d, dy], pass_r.at[d, dy], partner)
+
+    def each(start, stop, body):
+        lax.fori_loop(start, stop, lambda i, c: (body(i), c)[1], 0)
+
+    each(1, n, lambda d: hop(d).start())
+    rows_ref[me, :, mine] = out_ref[me]
+
+    def spread(d):
+        for dy in range(1, ys):
+            far(d, dy).start()
+        near(d).start()
+
+    def passing(d):
+        for dy in range(1, ys):
+            far(d, dy).wait_recv()
+            forward(d, dy).start()
+
+    spread(0)
+
+    def step(d):
+        hop(d).wait_recv()
+        spread(d)
+        passing(d - 1)
+
+    each(1, n, step)
+    passing(n - 1)
+
+    def finish(d):
+        near(d).wait()
+        for dy in range(1, ys):
+            far(d, dy).wait_send()
+            forward(d, dy).wait()
+
+    each(0, n, finish)
+    each(1, n, lambda d: hop(d).wait_send())
+
+
+def dispatch_rows(outgoing, n, tp_size):
+    _, capacity, width = outgoing.shape
+    ys = tp_size // 2
+    one, many = (n,), (n, ys)
+    sems = [pltpu.SemaphoreType.DMA(shape) for shape in (one, one, many, many) * 2]
+    return call(
+        functools.partial(dispatch_kernel, n, tp_size),
+        jax.ShapeDtypeStruct((n, capacity, width * tp_size), outgoing.dtype),
+        sems,
+        2,
+        outgoing,
+    )
+
+
+def combine_kernel(
+    n, tp_size, part_ref, back_ref, near, outbox, far, ready,
+    near_s, near_r, far_s, far_r, hop_s, hop_r,
+):
+    me, tp = lax.axis_index("sp"), lax.axis_index("tp")
+    ys = tp_size // 2
+    y, core = tp // 2, tp % 2
+    partner = (me, y * 2 + 1 - core)
+    width = back_ref.shape[2]
+    enter(
+        [((me + d) % n, tp) for d in range(1, n)]
+        + [(me, ((y + dy) % ys) * 2 + core) for dy in range(1, ys)]
+        + [partner]
+    )
+
+    def near_copy(i, dy):
+        block = (me + i + 1) % n
+        cols = tp_columns(((y + dy) % ys) * 2 + 1 - core, width)
+        return remote(
+            part_ref.at[block, :, cols], near.at[i, dy], near_s.at[i, dy], near_r.at[i, dy],
+            partner,
+        )
+
+    def far_copy(i, dy):
+        return remote(
+            outbox.at[i, dy], far.at[i, dy], far_s.at[i, dy], far_r.at[i, dy],
+            (me, ((y + dy) % ys) * 2 + core),
+        )
+
+    def hop_copy(i):
+        return remote(
+            ready.at[i], back_ref.at[me], hop_s.at[i], hop_r.at[i], ((me + i + 1) % n, tp)
+        )
+
+    def each(start, stop, body):
+        lax.fori_loop(start, stop, lambda i, c: (body(i), c)[1], 0)
+
+    def begin(i):
+        for dy in list(range(1, ys)) + [0]:
+            near_copy(i, dy).start()
+
+    def pair_sum(i, dy):
+        near_copy(i, dy).wait_recv()
+        own = part_ref[(me + i + 1) % n, :, tp_columns(((y + dy) % ys) * 2 + core, width)]
+        return own.astype(jnp.float32) + near[i, dy].astype(jnp.float32)
+
+    def across(i):
+        for dy in range(1, ys):
+            outbox[i, dy] = pair_sum(i, dy).astype(jnp.bfloat16)
+            far_copy(i, dy).start()
+
+    def total(i):
+        value = pair_sum(i, 0)
+        for dy in range(1, ys):
+            far_copy(i, dy).wait_recv()
+            value = value + far[i, dy].astype(jnp.float32)
+        return value.astype(jnp.bfloat16)
+
+    def deliver(i):
+        ready[i] = total(i)
+        hop_copy(i).start()
+
+    each(0, n, begin)
+    lag = min(2, n - 1)
+    each(0, lag, across)
+
+    def step(i):
+        across(i)
+        deliver(i - lag)
+
+    each(lag, n, step)
+    each(n - lag, n - 1, deliver)
+    back_ref[me] = total(n - 1)
+
+    def finish(i):
+        for dy in range(ys):
+            near_copy(i, dy).wait_send()
+        for dy in range(1, ys):
+            far_copy(i, dy).wait_send()
+
+    each(0, n, finish)
+    each(0, n - 1, lambda i: hop_copy(i).wait())
+
+
+def combine_rows(part, n, tp_size):
+    _, capacity, full = part.shape
+    width = full // tp_size
+    ys = tp_size // 2
+    many, one = (n, ys), (n,)
+    wide = many + (capacity, width)
+    return call(
+        functools.partial(combine_kernel, n, tp_size),
+        jax.ShapeDtypeStruct((n, capacity, width), part.dtype),
+        [pltpu.VMEM(wide, jnp.bfloat16)] * 3
+        + [pltpu.VMEM((n, capacity, width), jnp.bfloat16)]
+        + [pltpu.SemaphoreType.DMA(many)] * 4
+        + [pltpu.SemaphoreType.DMA(one)] * 2,
+        3,
+        part,
+    )
 
 
 def per_device(
@@ -104,7 +494,7 @@
         keys.reshape(tokens, pair_heads, head_dim), key_gain, cosine_table, sine_table
     )
     stacked = jnp.concatenate([key_rot.reshape(tokens, pair_width), values], axis=1)
-    own_tags = docs.astype(jnp.bfloat16)
+    own_tags = docs
     score_scale = head_dim ** (-0.5)
     stat_shape = (tokens, pair_heads, 2)
     initial = (
@@ -112,8 +502,10 @@
         jnp.zeros(stat_shape, jnp.float32),
         jnp.zeros(stat_shape + (head_dim,), jnp.float32),
     )
-    pair_rows = lax.all_gather(stacked, "sp", axis=0, tiled=True)
-    tag_rows = lax.all_gather(own_tags, "sp", axis=0, tiled=True)
+    groups, ranks = lax.axis_size("sp"), lax.axis_size("tp")
+    pair_rows, tag_rows = gather_blocks(stacked, docs, groups)
+    pair_rows = pair_rows.reshape(groups * tokens, 2 * pair_width)
+    tag_rows = tag_rows[:, 0].reshape(groups * tokens)
     length = pair_rows.shape[0]
     block_size = block_length(length)
     blocks = length // block_size
@@ -132,20 +524,8 @@
         .reshape(tokens, query_heads * head_dim)
     )
     width_local = residual.shape[1]
-    projected = lax.psum_scatter(
-        lax.dot_general(
-            out_weight, attended, (((0,), (1,)), ((), ())), preferred_element_type=jnp.float32
-        ).astype(jnp.bfloat16),
-        "tp",
-        scatter_dimension=0,
-        tiled=True,
-    ).astype(jnp.float32)
-    mixed_first = residual.astype(jnp.float32) + projected.T
-    squares = lax.psum(jnp.sum(mixed_first * mixed_first, axis=1), "tp")
-    full_width = width_local * lax.axis_size("tp")
-    normed = (mixed_first * lax.rsqrt(squares / full_width + EPSILON)[:, None] * norm_gain).astype(
-        jnp.bfloat16
-    )
+    part = jnp.dot(attended, out_weight, preferred_element_type=jnp.float32).astype(jnp.bfloat16)
+    mixed_first, normed = reduce_and_norm(part, residual, norm_gain, ranks)
     experts = lax.axis_size("sp")
     top_count = routes.shape[1]
     capacity = max(2, 5 * tokens * top_count // (4 * experts))
@@ -168,20 +548,15 @@
     down_local = down_weight[0]
     model_width = gate_local.shape[0]
     outgoing = jnp.where(occupied[..., None], normed[source_row], jnp.zeros((), jnp.bfloat16))
-    arrived = lax.all_to_all(outgoing, "sp", split_axis=0, concat_axis=0, tiled=True)
-    sources = arrived.shape[0]
-    flat_rows = arrived.reshape(-1, width_local)
-    column_piece = lax.all_gather(flat_rows, "tp", axis=1, tiled=True)
+    arrived = dispatch_rows(outgoing, groups, ranks)
+    column_piece = arrived.reshape(-1, model_width)
     gate_pre = jnp.dot(column_piece, gate_local, preferred_element_type=jnp.float32)
     up_pre = jnp.dot(column_piece, up_local, preferred_element_type=jnp.float32)
     hidden = clamped_unit(gate_pre, up_pre)
-    partial_value = jnp.dot(hidden, down_local, preferred_element_type=jnp.float32).reshape(
-        sources, capacity, model_width
-    )
-    expert_out = lax.psum_scatter(
-        partial_value.astype(jnp.bfloat16), "tp", scatter_dimension=2, tiled=True
-    )
-    returned = lax.all_to_all(expert_out, "sp", split_axis=0, concat_axis=0, tiled=True)
+    partial_value = jnp.dot(hidden, down_local, preferred_element_type=jnp.float32)
+    returned = combine_rows(
+        partial_value.astype(jnp.bfloat16).reshape(groups, capacity, model_width), groups, ranks
+    )
     lookup = flat_routes * capacity + slot_index
     picked = (
         returned.reshape(-1, width_local)[lookup]

time: 245 us -> 177 us (0.72)
  waiting for transfers between devices: 121 us -> 0 us
  Pallas kernels: 0 us -> 110 us
  blocking collectives: 51.2 us -> 0 us
  between operations: 13.6 us -> 0.45 us
  local copies, waits for them, and re-layouts: 14.6 us -> 21.7 us
  matrix products: 21.6 us -> 28.4 us
  starting transfers between devices: 5.82 us -> 0 us
    pallas_call x0 -> x4, Pallas kernels: none -> 110 us  [call(): pl.pallas_call(kernel, out_shape=out_shape, in_specs=[VMEM_SPEC] * len(ar...]
    reduce_scatter x2 -> x0, waiting for transfers between devices: 54.8 us -> none  [the longest x1 34.5 us: per_device(): lax.psum_scatter(partial_value.astype(jnp.bfloat16), 'tp', scatter_dimens...]
    all_gather x2 -> x0, waiting for transfers between devices: 49.8 us -> none  [the longest x1 26.5 us: per_device(): pair_rows = lax.all_gather(stacked, 'sp', axis=0, tiled=True)]
    all_to_all x1 -> x0, blocking collectives: 23.1 us -> none  [per_device(): lax.all_to_all(outgoing, 'sp', split_axis=0, concat_axis=0, tiled=True)]
    all_gather x1 -> x0, blocking collectives: 22.4 us -> none  [per_device(): tag_rows = lax.all_gather(own_tags, 'sp', axis=0, tiled=True)]
    all_to_all x1 -> x0, waiting for transfers between devices: 16.7 us -> none  [per_device(): lax.all_to_all(expert_out, 'sp', split_axis=0, concat_axis=0, tiled=True)]
    dot_general x1, matrix products: 4.18 us -> 12.7 us  [per_device(): jnp.dot(hidden, down_local, preferred_element_type=jnp.float32)]
    psum x1 -> x0, blocking collectives: 5.76 us -> none  [per_device(): squares = lax.psum(jnp.sum(mixed_first * mixed_first, axis=1), 'tp')]
  transfers between devices with their start and end apart: 5 -> 0, of which waited for: 5 -> 0; matrix products, arithmetic and copies ran while one was open for 3% -> 0% of each run, Pallas kernels for 0% -> 0%
where the time goes in v1:
time: 177 us; the launch traced here: 176 us
  Pallas kernels  110 us (62%)
  matrix products  28.4 us (16%)
  local copies, waits for them, and re-layouts  21.7 us (12%)
  other arithmetic  15.6 us (9%)
    pallas_call x4, Pallas kernels, call(): pl.pallas_call(kernel, out_shape=out_shape, in_specs=[VMEM_SPEC] * len(ar...  110 us
    dot_general x1, matrix products, per_device(): jnp.dot(hidden, down_local, preferred_element_type=jnp.float32)  12.7 us
    dot_general x1, matrix products, per_device(): up_pre = jnp.dot(column_piece, up_local, preferred_element_type=jnp.float32)  6.12 us
    slice x2, local copies, waits for them, and re-layouts, per_device(): pair_rows[:, :pair_width].reshape(blocks, block_size, pair_heads, head_dim)  4.1 us
    reduce_sum x1, other arithmetic, softmax_update(): denominator = denominator * factor + jnp.sum(weights, axis=-1)  4.05 us
    dot_general x1, matrix products, softmax_update(): jnp.einsum('tkgp,pkd->tkgd', weights.astype(jnp.bfloat16), value_block, p...  3.93 us
    dot_general x1, matrix products, softmax_update(): jnp.einsum('tkgd,pkd->tkgp', query_rot, key_block, preferred_element_type...  3.89 us
    gather x1, local copies, waits for them, and re-layouts, per_device(): returned.reshape(-1, width_local)[lookup]  3.81 us

profile of v1, /device:TPU:0, one launch (start us, length us, event | category | flops | bytes accessed | tf_op | source)
XLA Modules:
  0.0 176.3 jit_solution(11357235410375172005)
XLA Ops:
  0.0 0.0 copy-start
  0.0 1.1 copy.33
  1.2 0.1 reshape.372
  1.3 0.8 mul.220
  2.1 0.2 multiply_multiply_fusion.1
  2.4 0.1 broadcast_multiply_fusion.1
  2.4 0.1 fusion.33
  2.6 0.0 copy-start.5
  2.6 0.3 subtract_convert_fusion.1
  2.9 0.3 pad_maximum_fusion.2
  3.2 0.1 convert_element_type.81
  3.3 0.1 copy.34
  3.4 1.6 pad_maximum_fusion.kv_ref
  5.0 1.3 broadcast_in_dim.92.doc_ref
  6.3 36.1 %shard_map.136 = (bf16[8,256,512]{2,1,0:T(8,128)(2,1)}, s32[8,8,256]{2,1,0:T(8,128)}) custom-call(bf16[256,512]{1,0:T(8,128)(2,1)} %pad_maximum_fusion.kv_ref, s32[8,256]{1,0:T(8,128)} %broadcast_in_dim.92.doc_ref), custom_call_target="tpu_custom_call" | custom-call | tf_op jit(solution)/shard_map/pallas_call | solution.py:104
  42.4 0.0 copy-start.7
  42.4 2.7 %fusion.51 = (bf16[2048,256]{1,0:T(8,128)(2,1)S(1)}, bf16[2048,256]{1,0:T(8,128)(2,1)}) fusion(bf16[2048,512]{1,0:T(8,128)(2,1)} %bitcast.112), kind=kLoop, calls=%fused_computation.92 | loop fusion | bytes 4194304 | tf_op jit(solution)/shard_map/slice | solution.py:512
  45.0 2.3 %copy.37 = bf16[2048,256]{0,1:T(8,128)(2,1)} copy(bf16[2048,256]{1,0:T(8,128)(2,1)} %get-tuple-element.41) | data formatting | bytes 2097152 | tf_op jit(solution)/shard_map/slice | solution.py:513
  47.3 0.8 slice.29
  48.2 0.0 copy-done.5
  48.2 1.1 broadcast_compare_fusion
  49.3 1.4 copy.35
  50.7 1.1 copy.36
  51.9 0.3 reshape.373
  52.2 0.0 copy-done.7
  52.2 0.1 mul.239
  52.3 0.1 bitcast_reduce_fusion
  52.4 0.3 multiply_multiply_fusion
  52.6 0.7 subtract_convert_fusion
  53.3 0.6 pad_maximum_fusion.1
  53.9 0.1 convert_element_type.85
  54.0 0.0 copy-done.2
  54.0 3.9 %fusion = (f32[256,4,2]{0,2,1:T(2,128)S(1)}, f32[4,2048,256,2]{2,1,3,0:T(8,128)S(1)}) fusion(pred[256,2048]{0,1:T(8,128)(4,1)S(1)} %copy-done.2, bf16[2048,4,64,1]{0,2,3,1:T(8,128)(2,1)} %bitcast.114, bf16[256,4,2,64]{0,3,2,1:T(8,128)(2,1)S(1)} %convert_element_type.85), kind=kOutput, calls=%fused_computation.4 | convolution fusion | flops 549451776 | bytes 18620416 | tf_op jit(solution)/shard_map/while/body/eval_jaxpr/tkgd,pkd->tkgp/dot_general | solution.py:62
  57.9 0.0 copy-start.3
  58.0 4.0 %fusion.1 = f32[256,4,2]{0,2,1:T(2,128)S(1)} fusion(f32[4,2048,256,2]{2,1,3,0:T(8,128)S(1)} %get-tuple-element.53, f32[256,4,2]{0,2,1:T(2,128)S(1)} %broadcast_maximum_fusion, pred[256,2048]{0,1:T(8,128)(4,1)S(1)} %copy-done.2), kind=kLoop, calls=%fused_computation.5 | loop fusion | flops 20969472 | bytes 17317888 | tf_op jit(solution)/shard_map/while/body/eval_jaxpr/reduce_sum | solution.py:70
  62.0 0.0 copy-done.3
  62.0 3.9 %fusion.27 = bf16[256,4,2,64]{0,3,2,1:T(8,128)(2,1)S(1)} fusion(bf16[2048,4,64,1]{0,2,3,1:T(8,128)(2,1)S(1)} %bitcast.113, f32[4,2048,256,2]{2,1,3,0:T(8,128)S(1)} %get-tuple-element.53, f32[256,4,2]{0,2,1:T(2,128)S(1)} %broadcast_maximum_fusion, pred[256,2048]{0,1:T(8,128)(4,1)S(1)} %copy-done.2, f32[256,4,2]{0,2,1:T(2,128)S(1)} %get-tuple-element.49, ...), kind=kOutput, calls=%fused_computation.26 | convolution fusion | flops 558235648 | bytes 18636800 | tf_op jit(solution)/shard_map/while/body/eval_jaxpr/tkgp,pkd->tkgd/dot_general | solution.py:71
  66.0 0.0 copy-start.4
  66.0 1.7 convolution_convert_fusion.part_ref
  67.7 16.0 %shard_map.137 = (f32[256,512]{1,0:T(8,128)}, bf16[256,512]{1,0:T(8,128)(2,1)}) custom-call(bf16[256,2048]{1,0:T(8,128)(2,1)} %convolution_convert_fusion.part_ref, bf16[256,512]{1,0:T(8,128)(2,1)} %res_ref.1, f32[1,512]{1,0:T(1,128)} %bitcast.119), custom_call_target="tpu_custom_call" | custom-call | tf_op jit(solution)/shard_map/pallas_call | solution.py:104
  83.8 0.1 copy.40
  83.9 0.1 eq.92
  84.1 1.1 reduce-window.6
  85.2 0.2 slice_reduce_fusion
  85.5 0.1 eq.88
  85.6 0.1 fusion.35
  85.8 0.3 fusion.17
  86.1 0.1 reshape.377
  86.2 0.0 copy-done.1
  86.2 2.8 %gather_fusion = bf16[640,512]{1,0:T(8,128)(2,1)S(1)} fusion(bf16[256,512]{1,0:T(8,128)(2,1)S(1)} %copy-done.1, s32[1024]{0:T(1024)S(1)} %pad_clamp_fusion.1), kind=kCustom, calls=%fused_computation | custom fusion | bytes 1313280 | tf_op jit(solution)/shard_map/gather | solution.py:550
  89.0 0.0 copy-start.8
  89.0 0.2 and_reduce_fusion
  89.2 1.0 broadcast_select_fusion.out_ref
  90.2 29.5 %shard_map.138 = bf16[8,80,2048]{2,1,0:T(8,128)(2,1)} custom-call(bf16[8,80,512]{2,1,0:T(8,128)(2,1)} %broadcast_select_fusion.out_ref), custom_call_target="tpu_custom_call" | custom-call | tf_op jit(solution)/shard_map/pallas_call | solution.py:104
  119.7 6.1 %fusion.8 = f32[640,1024]{1,0:T(8,128)} fusion(bf16[640,2048]{1,0:T(8,128)(2,1)} %bitcast.108, bf16[1,2048,1024]{2,1,0:T(8,128)(2,1)S(1)} %copy-done.8), kind=kOutput, calls=%fused_computation.11 | convolution fusion | flops 2684354560 | bytes 9437184 | tf_op jit(solution)/shard_map/dot_general | solution.py:554
  125.8 12.7 %fusion.12 = bf16[640,2048]{1,0:T(8,128)(2,1)} fusion(bf16[1,1024,2048]{2,1,0:T(8,128)(2,1)} %param.27, f32[640,1024]{1,0:T(8,128)} %fusion.8, bf16[640,2048]{1,0:T(8,128)(2,1)} %bitcast.109, bf16[1,2048,1024]{2,1,0:T(8,128)(2,1)} %param.25), kind=kOutput, calls=%fused_computation.15 | convolution fusion | flops 5376573440 | bytes 16252928 | tf_op jit(solution)/shard_map/dot_general | solution.py:556
  138.5 28.6 %shard_map.139 = bf16[8,80,512]{2,1,0:T(8,128)(2,1)} custom-call(bf16[8,80,2048]{2,1,0:T(8,128)(2,1)} %bitcast.110), custom_call_target="tpu_custom_call" | custom-call | tf_op jit(solution)/shard_map/pallas_call | solution.py:104
  167.2 0.1 copy.42
  167.3 0.1 mul.260
  167.5 3.8 %gather_fusion.1 = bf16[512,512]{1,0:T(8,128)(2,1)} fusion(bf16[640,512]{1,0:T(8,128)(2,1)} %bitcast.107, s32[1024]{0:T(1024)S(1)} %pad_clamp_fusion), kind=kCustom, calls=%fused_computation.1 | custom fusion | bytes 1050624 | tf_op jit(solution)/shard_map/gather | solution.py:562
  171.3 1.7 reshape.374
  173.0 0.1 copy.39
  173.2 1.3 multiply_reduce_fusion
  174.5 1.8 %add_convert_fusion = bf16[256,512]{1,0:T(8,128)(2,1)} fusion(f32[256,512]{1,0:T(8,128)} %get-tuple-element.36, f32[256,512]{1,0:T(8,128)S(1)} %multiply_reduce_fusion), kind=kLoop, calls=%fused_computation.29 | loop fusion | flops 262144 | bytes 1310720 | tf_op jit(solution)/shard_map/convert_element_type | solution.py:567
  (24 shorter events, 0.2 us)
Async XLA Ops:
  0.0 66.0 %copy-start = (bf16[512,2048]{1,0:T(8,128)(2,1)S(1)}, bf16[512,2048]{1,0:T(8,128)(2,1)}, u32[]{:S(2)}) copy-start(bf16[512,2048]{1,0:T(8,128)(2,1)} %param.20) | copy-start | bytes 6291460
  2.6 45.6 %copy-start.5 = (s32[256]{0:T(256)S(1)}, s32[256]{0:T(256)}, u32[]{:S(2)}) copy-start(s32[256]{0:T(256)} %param.17) | copy-start | bytes 3076
  42.4 9.8 %copy-start.7 = (f32[64]{0:T(128)S(1)}, f32[64]{0:T(128)}, u32[]{:S(2)}) copy-start(f32[64]{0:T(128)} %param.18) | copy-start | bytes 772
  50.7 3.3 %copy-start.2 = (pred[256,2048]{0,1:T(8,128)(4,1)S(1)}, pred[256,2048]{0,1:T(8,128)(4,1)}, u32[]{:S(2)}) copy-start(pred[256,2048]{0,1:T(8,128)(4,1)} %broadcast_compare_fusion) | copy-start | bytes 1572868
  57.9 4.1 %copy-start.3 = (bf16[2048,256]{0,1:T(8,128)(2,1)S(1)}, bf16[2048,256]{0,1:T(8,128)(2,1)}, u32[]{:S(2)}) copy-start(bf16[2048,256]{0,1:T(8,128)(2,1)} %copy.37) | copy-start | bytes 3145732
  66.0 17.8 %copy-start.4 = (s32[256,2]{0,1:T(2,128)S(1)}, s32[256,2]{0,1:T(2,128)}, u32[]{:S(2)}) copy-start(s32[256,2]{0,1:T(2,128)} %param.23) | copy-start | bytes 6148
  83.8 2.4 %copy-start.1 = (bf16[256,512]{1,0:T(8,128)(2,1)S(1)}, bf16[256,512]{1,0:T(8,128)(2,1)}, u32[]{:S(2)}) copy-start(bf16[256,512]{1,0:T(8,128)(2,1)} %get-tuple-element.38) | copy-start | bytes 786436
  89.0 30.7 %copy-start.8 = (bf16[1,2048,1024]{2,1,0:T(8,128)(2,1)S(1)}, bf16[1,2048,1024]{2,1,0:T(8,128)(2,1)}, u32[]{:S(2)}) copy-start(bf16[1,2048,1024]{2,1,0:T(8,128)(2,1)} %param.26) | copy-start | bytes 12582916
  138.5 34.5 %copy-start.6 = (f32[256,2]{0,1:T(2,128)S(1)}, f32[256,2]{0,1:T(2,128)}, u32[]{:S(2)}) copy-start(f32[256,2]{0,1:T(2,128)} %param.24) | copy-start | bytes 6148

commit v2 on v1

--- a/solution.py
+++ b/solution.py
@@ -274,8 +274,11 @@
     )
 
 
-def dispatch_kernel(
-    n, tp_size, out_ref, rows_ref, hop_s, hop_r, far_s, far_r, near_s, near_r, pass_s, pass_r
+def expert_kernel(
+    n, tp_size, out_ref, gate_hbm, up_hbm, down_hbm, back_ref,
+    rows, gate, up, down, hidden, part, near, outbox, far, ready, load_sem,
+    in_s, in_r, side_s, side_r, back_s, back_r,
+    cross_s, cross_r, pass_s, pass_r, near_s, near_r, far_s, far_r,
 ):
     me, tp = lax.axis_index("sp"), lax.axis_index("tp")
     ys = tp_size // 2
@@ -283,184 +286,183 @@
     partner = (me, y * 2 + 1 - core)
     width = out_ref.shape[2]
     mine = tp_columns(tp, width)
+    loads = [
+        pltpu.make_async_copy(src.at[0], dst, load_sem.at[i])
+        for i, (src, dst) in enumerate(((gate_hbm, gate), (up_hbm, up), (down_hbm, down)))
+    ]
+    for load in loads:
+        load.start()
     enter(
         [((me + d) % n, tp) for d in range(1, n)]
         + [(me, ((y + dy) % ys) * 2 + core) for dy in range(1, ys)]
         + [partner]
     )
 
-    def hop(d):
+    def source(d):
+        return (me - d + n) % n
+
+    def across_y(dy):
+        return (me, ((y + dy) % ys) * 2 + core)
+
+    def hop_in(d):
         peer = (me + d) % n
         return remote(
-            out_ref.at[peer], rows_ref.at[me, :, mine], hop_s.at[d], hop_r.at[d], (peer, tp)
-        )
-
-    def far(d, dy):
-        block = (me - d + n) % n
-        view = rows_ref.at[block, :, mine]
-        return remote(
-            view, view, far_s.at[d, dy], far_r.at[d, dy], (me, ((y + dy) % ys) * 2 + core)
-        )
-
-    def near(d):
-        view = rows_ref.at[(me - d + n) % n, :, mine]
-        return remote(view, view, near_s.at[d], near_r.at[d], partner)
+            out_ref.at[peer], rows.at[me, :, mine], in_s.at[d], in_r.at[d], (peer, tp)
+        )
+
+    def cross(d, dy):
+        view = rows.at[source(d), :, mine]
+        return remote(view, view, cross_s.at[d, dy], cross_r.at[d, dy], across_y(dy))
+
+    def side(d):
+        view = rows.at[source(d), :, mine]
+        return remote(view, view, side_s.at[d], side_r.at[d], partner)
 
     def forward(d, dy):
         origin = ((y - dy + ys) % ys) * 2 + core
-        view = rows_ref.at[(me - d + n) % n, :, tp_columns(origin, width)]
+        view = rows.at[source(d), :, tp_columns(origin, width)]
         return remote(view, view, pass_s.at[d, dy], pass_r.at[d, dy], partner)
+
+    def near_copy(d, dy):
+        cols = tp_columns(((y + dy) % ys) * 2 + 1 - core, width)
+        return remote(
+            part.at[d, :, cols], near.at[d, dy], near_s.at[d, dy], near_r.at[d, dy], partner
+        )
+
+    def far_copy(d, dy):
+        return remote(
+            outbox.at[d, dy], far.at[d, dy], far_s.at[d, dy], far_r.at[d, dy], across_y(dy)
+        )
+
+    def hop_back(d):
+        return remote(
+            ready.at[d], back_ref.at[me], back_s.at[d], back_r.at[d], (source(d), tp)
+        )
 
     def each(start, stop, body):
         lax.fori_loop(start, stop, lambda i, c: (body(i), c)[1], 0)
 
-    each(1, n, lambda d: hop(d).start())
-    rows_ref[me, :, mine] = out_ref[me]
-
     def spread(d):
+        @pl.when(d > 0)
+        def _():
+            hop_in(d).wait_recv()
+
         for dy in range(1, ys):
-            far(d, dy).start()
-        near(d).start()
-
-    def passing(d):
+            cross(d, dy).start()
+        side(d).start()
+
+    def relay(d):
         for dy in range(1, ys):
-            far(d, dy).wait_recv()
+            cross(d, dy).wait_recv()
             forward(d, dy).start()
 
-    spread(0)
-
-    def step(d):
-        hop(d).wait_recv()
-        spread(d)
-        passing(d - 1)
-
-    each(1, n, step)
-    passing(n - 1)
+    def compute(d):
+        @pl.when(d == 0)
+        def _():
+            for load in loads:
+                load.wait()
+
+        side(d).wait_recv()
+        for dy in range(1, ys):
+            forward(d, dy).wait_recv()
+        block = rows[source(d)]
+        units = gate.shape[1]
+        piece = min(256, units)
+        for start in range(0, units, piece):
+            span = slice(start, start + piece)
+            gate_pre = jnp.dot(block, gate[:, span], preferred_element_type=jnp.float32)
+            up_pre = jnp.dot(block, up[:, span], preferred_element_type=jnp.float32)
+            hidden[:, span] = clamped_unit(gate_pre, up_pre)
+        units_in = hidden[...]
+        for t in range(tp_size):
+            span = slice(t * width, (t + 1) * width)
+            part[d, :, span] = jnp.dot(
+                units_in, down[:, span], preferred_element_type=jnp.float32
+            ).astype(jnp.bfloat16)
+        for dy in list(range(1, ys)) + [0]:
+            near_copy(d, dy).start()
+
+    def pair_sum(d, dy):
+        near_copy(d, dy).wait_recv()
+        own = part[d, :, tp_columns(((y + dy) % ys) * 2 + core, width)]
+        return own.astype(jnp.float32) + near[d, dy].astype(jnp.float32)
+
+    def reduce_pair(d):
+        for dy in range(1, ys):
+            outbox[d, dy] = pair_sum(d, dy).astype(jnp.bfloat16)
+            far_copy(d, dy).start()
+
+    def deliver(d):
+        value = pair_sum(d, 0)
+        for dy in range(1, ys):
+            far_copy(d, dy).wait_recv()
+            value = value + far[d, dy].astype(jnp.float32)
+        ready[d] = value.astype(jnp.bfloat16)
+
+        @pl.when(d > 0)
+        def _():
+            hop_back(d).start()
+
+    stages = ((spread, 0), (relay, 1), (reduce_pair, 3), (deliver, 4), (compute, 2))
+
+    def step(k):
+        for stage, lag in stages:
+            @pl.when((k >= lag) & (k < n + lag))
+            def _(stage=stage, lag=lag):
+                stage(k - lag)
+
+    each(1, n, lambda d: hop_in(d).start())
+    rows[me, :, mine] = out_ref[me]
+    each(0, n + 4, step)
+    back_ref[me] = ready[0]
 
     def finish(d):
-        near(d).wait()
+        side(d).wait_send()
         for dy in range(1, ys):
-            far(d, dy).wait_send()
-            forward(d, dy).wait()
+            cross(d, dy).wait_send()
+            forward(d, dy).wait_send()
+            far_copy(d, dy).wait_send()
+        for dy in range(ys):
+            near_copy(d, dy).wait_send()
+
+    def finish_hops(d):
+        hop_in(d).wait_send()
+        hop_back(d).wait()
 
     each(0, n, finish)
-    each(1, n, lambda d: hop(d).wait_send())
-
-
-def dispatch_rows(outgoing, n, tp_size):
+    each(1, n, finish_hops)
+
+
+def run_experts(outgoing, gate_weight, up_weight, down_weight, n, tp_size):
     _, capacity, width = outgoing.shape
     ys = tp_size // 2
-    one, many = (n,), (n, ys)
-    sems = [pltpu.SemaphoreType.DMA(shape) for shape in (one, one, many, many) * 2]
-    return call(
-        functools.partial(dispatch_kernel, n, tp_size),
-        jax.ShapeDtypeStruct((n, capacity, width * tp_size), outgoing.dtype),
-        sems,
-        2,
-        outgoing,
-    )
-
-
-def combine_kernel(
-    n, tp_size, part_ref, back_ref, near, outbox, far, ready,
-    near_s, near_r, far_s, far_r, hop_s, hop_r,
-):
-    me, tp = lax.axis_index("sp"), lax.axis_index("tp")
-    ys = tp_size // 2
-    y, core = tp // 2, tp % 2
-    partner = (me, y * 2 + 1 - core)
-    width = back_ref.shape[2]
-    enter(
-        [((me + d) % n, tp) for d in range(1, n)]
-        + [(me, ((y + dy) % ys) * 2 + core) for dy in range(1, ys)]
-        + [partner]
-    )
-
-    def near_copy(i, dy):
-        block = (me + i + 1) % n
-        cols = tp_columns(((y + dy) % ys) * 2 + 1 - core, width)
-        return remote(
-            part_ref.at[block, :, cols], near.at[i, dy], near_s.at[i, dy], near_r.at[i, dy],
-            partner,
-        )
-
-    def far_copy(i, dy):
-        return remote(
-            outbox.at[i, dy], far.at[i, dy], far_s.at[i, dy], far_r.at[i, dy],
-            (me, ((y + dy) % ys) * 2 + core),
-        )
-
-    def hop_copy(i):
-        return remote(
-            ready.at[i], back_ref.at[me], hop_s.at[i], hop_r.at[i], ((me + i + 1) % n, tp)
-        )
-
-    def each(start, stop, body):
-        lax.fori_loop(start, stop, lambda i, c: (body(i), c)[1], 0)
-
-    def begin(i):
-        for dy in list(range(1, ys)) + [0]:
-            near_copy(i, dy).start()
-
-    def pair_sum(i, dy):
-        near_copy(i, dy).wait_recv()
-        own = part_ref[(me + i + 1) % n, :, tp_columns(((y + dy) % ys) * 2 + core, width)]
-        return own.astype(jnp.float32) + near[i, dy].astype(jnp.float32)
-
-    def across(i):
-        for dy in range(1, ys):
-            outbox[i, dy] = pair_sum(i, dy).astype(jnp.bfloat16)
-            far_copy(i, dy).start()
-
-    def total(i):
-        value = pair_sum(i, 0)
-        for dy in range(1, ys):
-            far_copy(i, dy).wait_recv()
-            value = value + far[i, dy].astype(jnp.float32)
-        return value.astype(jnp.bfloat16)
-
-    def deliver(i):
-        ready[i] = total(i)
-        hop_copy(i).start()
-
-    each(0, n, begin)
-    lag = min(2, n - 1)
-    each(0, lag, across)
-
-    def step(i):
-        across(i)
-        deliver(i - lag)
-
-    each(lag, n, step)
-    each(n - lag, n - 1, deliver)
-    back_ref[me] = total(n - 1)
-
-    def finish(i):
-        for dy in range(ys):
-            near_copy(i, dy).wait_send()
-        for dy in range(1, ys):
-            far_copy(i, dy).wait_send()
-
-    each(0, n, finish)
-    each(0, n - 1, lambda i: hop_copy(i).wait())
-
-
-def combine_rows(part, n, tp_size):
-    _, capacity, full = part.shape
-    width = full // tp_size
-    ys = tp_size // 2
-    many, one = (n, ys), (n,)
-    wide = many + (capacity, width)
-    return call(
-        functools.partial(combine_kernel, n, tp_size),
-        jax.ShapeDtypeStruct((n, capacity, width), part.dtype),
-        [pltpu.VMEM(wide, jnp.bfloat16)] * 3
-        + [pltpu.VMEM((n, capacity, width), jnp.bfloat16)]
-        + [pltpu.SemaphoreType.DMA(many)] * 4
-        + [pltpu.SemaphoreType.DMA(one)] * 2,
-        3,
-        part,
-    )
+    full, units = gate_weight.shape[1:]
+    wide = (n, ys, capacity, width)
+    kind = outgoing.dtype
+    shapes = [
+        (n, capacity, full),
+        (full, units),
+        (full, units),
+        (units, full),
+        (capacity, units),
+        (n, capacity, full),
+        wide,
+        wide,
+        wide,
+        (n, capacity, width),
+    ]
+    sems = [(3,)] + [(n,)] * 6 + [(n, ys)] * 8
+    return pl.pallas_call(
+        functools.partial(expert_kernel, n, tp_size),
+        out_shape=jax.ShapeDtypeStruct((n, capacity, width), kind),
+        in_specs=[VMEM_SPEC] + [pl.BlockSpec(memory_space=pl.ANY)] * 3,
+        out_specs=VMEM_SPEC,
+        scratch_shapes=[pltpu.VMEM(shape, kind) for shape in shapes]
+        + [pltpu.SemaphoreType.DMA(shape) for shape in sems],
+        compiler_params=pltpu.CompilerParams(
+            collective_id=2, has_side_effects=True, vmem_limit_bytes=VMEM_LIMIT
+        ),
+    )(outgoing, gate_weight, up_weight, down_weight)
 
 
 def per_device(
@@ -535,35 +537,22 @@
     onehot = (flat_routes[:, None] == expert_ids[None, :]).astype(jnp.int32)
     earlier = jnp.cumsum(onehot, axis=0) - onehot
     slot_index = jnp.sum(earlier * onehot, axis=1)
-    slot_ids = jnp.arange(capacity, dtype=jnp.int32)
-    matches = (flat_routes[:, None, None] == expert_ids[None, :, None]) & (
-        slot_index[:, None, None] == slot_ids[None, None, :]
-    )
-    entry_ids = jnp.arange(entries, dtype=jnp.int32)
-    source_entry = jnp.sum(jnp.where(matches, entry_ids[:, None, None], 0), axis=0)
-    occupied = jnp.any(matches, axis=0)
-    source_row = source_entry // top_count
-    gate_local = gate_weight[0]
-    up_local = up_weight[0]
-    down_local = down_weight[0]
-    model_width = gate_local.shape[0]
-    outgoing = jnp.where(occupied[..., None], normed[source_row], jnp.zeros((), jnp.bfloat16))
-    arrived = dispatch_rows(outgoing, groups, ranks)
-    column_piece = arrived.reshape(-1, model_width)
-    gate_pre = jnp.dot(column_piece, gate_local, preferred_element_type=jnp.float32)
-    up_pre = jnp.dot(column_piece, up_local, preferred_element_type=jnp.float32)
-    hidden = clamped_unit(gate_pre, up_pre)
-    partial_value = jnp.dot(hidden, down_local, preferred_element_type=jnp.float32)
-    returned = combine_rows(
-        partial_value.astype(jnp.bfloat16).reshape(groups, capacity, model_width), groups, ranks
-    )
-    lookup = flat_routes * capacity + slot_index
-    picked = (
-        returned.reshape(-1, width_local)[lookup]
-        .reshape(tokens, top_count, width_local)
-        .astype(jnp.float32)
-    )
-    routed = jnp.sum(route_weight[:, :, None] * picked, axis=1)
+    lookup = (flat_routes * capacity + slot_index).reshape(tokens, top_count)
+    slot_ids = jnp.arange(experts * capacity, dtype=jnp.int32)
+    holds = lookup[:, :, None] == slot_ids[None, None, :]
+    chosen = jnp.any(holds, axis=1).astype(jnp.bfloat16)
+    mixing = jnp.sum(jnp.where(holds, route_weight[:, :, None], 0.0), axis=1)
+    mixing_high = lax.reduce_precision(mixing, 8, 7)
+    mixing_low = (mixing - mixing_high).astype(jnp.bfloat16)
+    mixing_high = mixing_high.astype(jnp.bfloat16)
+    outgoing = lax.dot_general(
+        chosen, normed, (((0,), (0,)), ((), ())), preferred_element_type=jnp.float32
+    ).astype(jnp.bfloat16).reshape(experts, capacity, width_local)
+    returned = run_experts(outgoing, gate_weight, up_weight, down_weight, groups, ranks)
+    returned = returned.reshape(experts * capacity, width_local)
+    routed = jnp.dot(mixing_high, returned, preferred_element_type=jnp.float32) + jnp.dot(
+        mixing_low, returned, preferred_element_type=jnp.float32
+    )
     return (mixed_first + routed).astype(jnp.bfloat16)
 
 

time: 177 us -> 148 us (0.84)
  matrix products: 28.4 us -> 15.5 us
  local copies, waits for them, and re-layouts: 21.7 us -> 13.8 us
  Pallas kernels: 110 us -> 106 us
  other arithmetic: 15.6 us -> 11.9 us
    pallas_call x4 -> x2, Pallas kernels: 110 us -> 52 us  [call(): pl.pallas_call(kernel, out_shape=out_shape, in_specs=[VMEM_SPEC] * len(ar...]
    pallas_call x0 -> x1, Pallas kernels: none -> 53.5 us  [run_experts(): pl.pallas_call(functools.partial(expert_kernel, n, tp_size), out_shape=ja...]
    dot_general x2 -> x3, matrix products: 18.8 us -> 5.8 us  [the longest x1 2.18 us: per_device(): jnp.dot(mixing_low, returned, preferred_element_type=jnp.float32)]
    gather x2 -> x0, local copies, waits for them, and re-layouts: 6.6 us -> none  [the longest x1 3.81 us: per_device(): returned.reshape(-1, width_local)[lookup]]
    convert_element_type x1 -> x0, other arithmetic: 1.82 us -> none  [per_device(): return (mixed_first + routed).astype(jnp.bfloat16)]
where the time goes in v2:
time: 148 us; the launch traced here: 147 us
  Pallas kernels  106 us (72%)
  matrix products  15.5 us (10%)
  local copies, waits for them, and re-layouts  13.8 us (9%)
  other arithmetic  11.9 us (8%)
    pallas_call x1, Pallas kernels, run_experts(): pl.pallas_call(functools.partial(expert_kernel, n, tp_size), out_shape=ja...  53.5 us
    pallas_call x2, Pallas kernels, call(): pl.pallas_call(kernel, out_shape=out_shape, in_specs=[VMEM_SPEC] * len(ar...  52 us
    slice x2, local copies, waits for them, and re-layouts, per_device(): pair_rows[:, :pair_width].reshape(blocks, block_size, pair_heads, head_dim)  4.1 us
    dot_general x1, matrix products, softmax_update(): jnp.einsum('tkgd,pkd->tkgp', query_rot, key_block, preferred_element_type...  4.06 us
    reduce_sum x1, other arithmetic, softmax_update(): denominator = denominator * factor + jnp.sum(weights, axis=-1)  4.05 us
    dot_general x1, matrix products, softmax_update(): jnp.einsum('tkgp,pkd->tkgd', weights.astype(jnp.bfloat16), value_block, p...  3.93 us

profile of v2, /device:TPU:0, one launch (start us, length us, event | category | flops | bytes accessed | tf_op | source)
XLA Modules:
  0.0 147.1 jit_solution(17186989311429112733)
XLA Ops:
  0.0 0.0 copy-start
  0.0 1.1 copy.45
  1.2 0.1 reshape.235
  1.3 0.8 mul.192
  2.1 0.2 multiply_multiply_fusion.1
  2.4 0.1 broadcast_multiply_fusion.1
  2.4 0.1 fusion.25
  2.6 0.3 subtract_convert_fusion.1
  2.9 0.3 pad_maximum_fusion.2
  3.2 0.1 convert_element_type.79
  3.3 0.1 copy.46
  3.4 1.6 %pad_maximum_fusion.kv_ref = bf16[256,512]{1,0:T(8,128)(2,1)} fusion(bf16[256,256]{1,0:T(8,128)(2,1)} %param.16, bf16[256,256]{1,0:T(8,128)(2,1)S(1)} %copy.46), kind=kLoop, calls=%fused_computation.26 | loop fusion | flops 524288 | bytes 524288 | tf_op jit(solution)/shard_map/concatenate | solution.py:498
  5.0 1.3 broadcast_in_dim.74.doc_ref
  6.3 36.1 %shard_map.136 = (bf16[8,256,512]{2,1,0:T(8,128)(2,1)}, s32[8,8,256]{2,1,0:T(8,128)}) custom-call(bf16[256,512]{1,0:T(8,128)(2,1)} %pad_maximum_fusion.kv_ref, s32[8,256]{1,0:T(8,128)} %broadcast_in_dim.74.doc_ref), custom_call_target="tpu_custom_call" | custom-call | tf_op jit(solution)/shard_map/pallas_call | solution.py:104
  42.3 2.7 %fusion.36 = (bf16[2048,256]{1,0:T(8,128)(2,1)S(1)}, bf16[2048,256]{1,0:T(8,128)(2,1)}) fusion(bf16[2048,512]{1,0:T(8,128)(2,1)} %bitcast.75), kind=kLoop, calls=%fused_computation.69 | loop fusion | bytes 4194304 | tf_op jit(solution)/shard_map/slice | solution.py:514
  45.0 2.3 %copy.49 = bf16[2048,256]{0,1:T(8,128)(2,1)} copy(bf16[2048,256]{1,0:T(8,128)(2,1)} %get-tuple-element.41) | data formatting | bytes 2097152 | tf_op jit(solution)/shard_map/slice | solution.py:515
  47.3 0.8 slice.29
  48.1 1.8 %broadcast_compare_fusion = pred[256,2048]{0,1:T(8,128)(4,1)} fusion(s32[256]{0:T(256)} %param.17, s32[2048]{0:T(1024)S(1)} %bitcast.79), kind=kLoop, calls=%fused_computation.17 | loop fusion | flops 524288 | bytes 533504 | tf_op jit(solution)/shard_map/while/body/eval_jaxpr/eq | solution.py:65
  49.9 1.4 copy.47
  51.4 0.0 copy-start.1
  51.4 1.1 copy.48
  52.5 0.3 reshape.236
  52.8 0.8 mul.211
  53.6 0.1 bitcast_reduce_fusion
  53.6 0.3 multiply_multiply_fusion
  53.9 0.7 subtract_convert_fusion
  54.6 0.6 pad_maximum_fusion.1
  55.2 0.1 convert_element_type.83
  55.3 0.0 copy-start.2
  55.3 4.1 %fusion = (f32[256,4,2]{0,2,1:T(2,128)S(1)}, f32[4,2048,256,2]{2,1,3,0:T(8,128)S(1)}) fusion(pred[256,2048]{0,1:T(8,128)(4,1)} %broadcast_compare_fusion, bf16[2048,4,64,1]{0,2,3,1:T(8,128)(2,1)} %bitcast.77, bf16[256,4,2,64]{0,3,2,1:T(8,128)(2,1)S(1)} %convert_element_type.83), kind=kOutput, calls=%fused_computation.2 | convolution fusion | flops 549451776 | bytes 18620416 | tf_op jit(solution)/shard_map/while/body/eval_jaxpr/tkgd,pkd->tkgp/dot_general | solution.py:62
  59.4 0.0 copy-done.1
  59.4 4.0 %fusion.1 = f32[256,4,2]{0,2,1:T(2,128)S(1)} fusion(f32[4,2048,256,2]{2,1,3,0:T(8,128)S(1)} %get-tuple-element.53, f32[256,4,2]{0,2,1:T(2,128)S(1)} %broadcast_maximum_fusion, pred[256,2048]{0,1:T(8,128)(4,1)S(1)} %copy-done.1), kind=kLoop, calls=%fused_computation.3 | loop fusion | flops 20969472 | bytes 17317888 | tf_op jit(solution)/shard_map/while/body/eval_jaxpr/reduce_sum | solution.py:70
  63.5 0.0 copy-done.2
  63.5 0.0 copy-start.4
  63.5 3.9 %fusion.18 = bf16[256,4,2,64]{0,3,2,1:T(8,128)(2,1)S(1)} fusion(bf16[2048,4,64,1]{0,2,3,1:T(8,128)(2,1)S(1)} %bitcast.76, f32[4,2048,256,2]{2,1,3,0:T(8,128)S(1)} %get-tuple-element.53, f32[256,4,2]{0,2,1:T(2,128)S(1)} %broadcast_maximum_fusion, pred[256,2048]{0,1:T(8,128)(4,1)S(1)} %copy-done.1, f32[256,4,2]{0,2,1:T(2,128)S(1)} %get-tuple-element.49, ...), kind=kOutput, calls=%fused_computation.19 | convolution fusion | flops 558235648 | bytes 18636800 | tf_op jit(solution)/shard_map/while/body/eval_jaxpr/tkgp,pkd->tkgd/dot_general | solution.py:71
  67.5 0.0 copy-start.5
  67.5 0.0 copy-done
  67.5 1.7 %convolution_convert_fusion.part_ref = bf16[256,2048]{1,0:T(8,128)(2,1)} fusion(bf16[256,512]{0,1:T(8,128)(2,1)S(1)} %bitcast.78, bf16[512,2048]{1,0:T(8,128)(2,1)S(1)} %copy-done), kind=kOutput, calls=%fused_computation.7 | convolution fusion | flops 537395200 | bytes 3407872 | tf_op jit(solution)/shard_map/dot_general | solution.py:529
  69.2 16.0 %shard_map.137 = (f32[256,512]{1,0:T(8,128)}, bf16[256,512]{1,0:T(8,128)(2,1)}) custom-call(bf16[256,2048]{1,0:T(8,128)(2,1)} %convolution_convert_fusion.part_ref, bf16[256,512]{1,0:T(8,128)(2,1)} %res_ref.1, f32[1,512]{1,0:T(1,128)} %bitcast.80), custom_call_target="tpu_custom_call" | custom-call | tf_op jit(solution)/shard_map/pallas_call | solution.py:104
  85.2 0.0 copy-start.3
  85.2 0.0 copy-done.4
  85.2 0.1 copy.51
  85.3 0.1 eq.75
  85.5 1.1 reduce-window.6
  86.6 0.2 slice_reduce_fusion
  86.9 0.1 eq.71
  87.0 0.1 fusion.27
  87.1 0.1 reduce_sum.52
  87.3 0.1 copy.53
  87.4 0.2 fusion.6
  87.6 2.2 %convolution_convert_fusion.1 = bf16[640,512]{1,0:T(8,128)(2,1)} fusion(pred[256,640]{1,0:T(8,128)(4,1)S(1)} %fusion.6, bf16[256,512]{1,0:T(8,128)(2,1)} %get-tuple-element.38), kind=kOutput, calls=%fused_computation.8 | convolution fusion | flops 168099840 | bytes 1081344 | tf_op jit(solution)/shard_map/dot_general | solution.py:548
  89.7 53.5 %shard_map.138 = bf16[8,80,512]{2,1,0:T(8,128)(2,1)} custom-call(bf16[8,80,512]{2,1,0:T(8,128)(2,1)} %bitcast.74, bf16[1,2048,1024]{2,1,0:T(8,128)(2,1)} %gate_hbm.1, bf16[1,2048,1024]{2,1,0:T(8,128)(2,1)} %up_hbm.1, bf16[1,1024,2048]{2,1,0:T(8,128)(2,1)} %down_hbm.1), custom_call_target="tpu_custom_call" | custom-call | tf_op jit(solution)/shard_map/pallas_call | solution.py:455
  143.3 0.0 copy-done.5
  143.3 0.2 select_reduce_fusion
  143.5 1.4 fusion.23
  144.9 0.0 copy-done.3
  144.9 2.2 %fusion.14 = bf16[256,512]{1,0:T(8,128)(2,1)} fusion(f32[256,512]{1,0:T(8,128)S(1)} %copy-done.3, f32[256,512]{1,0:T(8,128)S(1)} %fusion.23, bf16[640,512]{1,0:T(8,128)(2,1)} %bitcast.73, f32[256,640]{1,0:T(8,128)S(1)} %select_reduce_fusion), kind=kOutput, calls=%fused_computation.16 | convolution fusion | flops 168656896 | bytes 2621440 | tf_op jit(solution)/shard_map/dot_general | solution.py:553
  (11 shorter events, 0.2 us)
Async XLA Ops:
  0.0 67.5 %copy-start = (bf16[512,2048]{1,0:T(8,128)(2,1)S(1)}, bf16[512,2048]{1,0:T(8,128)(2,1)}, u32[]{:S(2)}) copy-start(bf16[512,2048]{1,0:T(8,128)(2,1)} %param.20) | copy-start | bytes 6291460
  51.4 8.0 %copy-start.1 = (pred[256,2048]{0,1:T(8,128)(4,1)S(1)}, pred[256,2048]{0,1:T(8,128)(4,1)}, u32[]{:S(2)}) copy-start(pred[256,2048]{0,1:T(8,128)(4,1)} %broadcast_compare_fusion) | copy-start | bytes 1572868
  55.3 8.2 %copy-start.2 = (bf16[2048,256]{0,1:T(8,128)(2,1)S(1)}, bf16[2048,256]{0,1:T(8,128)(2,1)}, u32[]{:S(2)}) copy-start(bf16[2048,256]{0,1:T(8,128)(2,1)} %copy.49) | copy-start | bytes 3145732
  63.5 21.7 %copy-start.4 = (s32[256,2]{0,1:T(2,128)S(1)}, s32[256,2]{0,1:T(2,128)}, u32[]{:S(2)}) copy-start(s32[256,2]{0,1:T(2,128)} %param.23) | copy-start | bytes 6148
  67.5 75.8 %copy-start.5 = (f32[256,2]{0,1:T(2,128)S(1)}, f32[256,2]{0,1:T(2,128)}, u32[]{:S(2)}) copy-start(f32[256,2]{0,1:T(2,128)} %param.24) | copy-start | bytes 6148
  85.2 59.8 %copy-start.3 = (f32[256,512]{1,0:T(8,128)S(1)}, f32[256,512]{1,0:T(8,128)}, u32[]{:S(2)}) copy-start(f32[256,512]{1,0:T(8,128)} %get-tuple-element.36) | copy-start | bytes 1572868
